TPU v7x, 32 devices: a whole 2x2x4 slice. The times are simulated.
32 devices in a mesh: ep: 8 (over z, core), tp: 4 (over y, x).
Axes of the slice: x: 2, y: 2, z: 4, core: 2. Of those that a mesh axis runs over, the one named last changes fastest.
Arguments:
- receptance: bfloat16 [2048, 2048], P('ep', 'tp'), may hold values from -6 to 6
- key_in: bfloat16 [2048, 2048], P('ep', 'tp'), may hold values from -6 to 6
- value_in: bfloat16 [2048, 2048], P('ep', 'tp'), may hold values from -6 to 6
- decay_in: bfloat16 [2048, 2048], P('ep', 'tp'), may hold values from -16 to 2
- rate_in: bfloat16 [2048, 2048], P('ep', 'tp'), may hold values from -12 to 4
- norm_gain: float32 [2048], P('tp'), may hold values from 0.1 to 1.9
- out_weight: bfloat16 [2048, 4096], P('tp'), may hold values from -0.125 to 0.125
- moe_in: bfloat16 [1024, 4096], P('ep'), may hold values from -6 to 6
- ffn_gain: float32 [4096], replicated, may hold values from 0.1 to 1.9
- routes: int32 [1024, 4], P('ep'), may hold values from 0 to 7, all different within a row; in each aligned block of 128 rows (0 to 127, 128 to 255, ...) at most 80 rows name the same one
- route_weights: float32 [1024, 4], P('ep'), may hold values from 0.2 to 1
- gate_weight: bfloat16 [8, 4096, 1024], P('ep', None, 'tp'), may hold values from -0.09375 to 0.09375
- up_weight: bfloat16 [8, 4096, 1024], P('ep', None, 'tp'), may hold values from -0.09375 to 0.09375
- down_weight: bfloat16 [8, 1024, 4096], P('ep', None, 'tp'), may hold values from -0.1875 to 0.1875
Outputs:
- mixer_out: bfloat16 [2048, 4096], P(('ep', 'tp'))
- moe_out: bfloat16 [1024, 4096], P('ep', 'tp')
Inputs may be any that keep to these rules, and one draw needn't show every extreme that they name: `routes`: A row names 4 different experts. Among the 128 rows that one index of ep holds, no expert is named by more than 80 rows, and in every draw some expert is named by exactly 80 of them.
All inputs are finite; a program needn't handle non-finite values.
Results may differ from a plain program's by a relative error of at most 0.025.
Values may be sent and summed in bfloat16 or wider, within the bound.
A program may use at most 64 MiB of HBM per device.

v0:
```python
import functools

import jax
import jax.numpy as jnp
from jax import lax
from jax.experimental import pallas as pl
from jax.experimental.pallas import tpu as pltpu
from jax.sharding import PartitionSpec as P

HD = 64
BLOCK = 64
F32 = jnp.float32
BF16 = jnp.bfloat16
MESH = pl.DeviceIdType.MESH


def dot(a, b):
    return jnp.dot(a.astype(BF16), b.astype(BF16), preferred_element_type=F32)


def dot_rows(a, b):
    return lax.dot_general(
        a.astype(BF16), b.astype(BF16), (((1,), (1,)), ((), ())), preferred_element_type=F32
    )


def dot_cols(a, b):
    return lax.dot_general(
        a.astype(BF16), b.astype(BF16), (((0,), (0,)), ((), ())), preferred_element_type=F32
    )


def dot_exact(a, b):
    return jnp.dot(a, b, precision=lax.Precision.HIGHEST, preferred_element_type=F32)


def lane_head(rows, width):
    return lax.broadcasted_iota(jnp.int32, (rows, width), 1) // HD


def spread(packed):
    rows, width = packed.shape
    packed = packed.astype(BF16)
    head = lane_head(rows, width)
    return jnp.concatenate(
        [jnp.where(head == i, packed, jnp.zeros_like(packed)) for i in range(width // HD)], axis=0
    )


def fold(square):
    width = square.shape[1]
    head = lane_head(HD, width)
    out = jnp.zeros((HD, width), F32)
    for i in range(width // HD):
        out = jnp.where(head == i, square[i * HD : (i + 1) * HD], out)
    return out


def head_ones(width):
    row = lax.broadcasted_iota(jnp.int32, (width, width), 0) // HD
    return (row == lane_head(width, width)).astype(F32)


def group_width(columns):
    return HD * max(g for g in (4, 2, 1) if columns % (g * HD) == 0)


def tables_kernel(r_ref, k_ref, v_ref, d_ref, a_ref, read_ref, local_ref, total_ref, carry):
    columns = r_ref.shape[1]
    width = group_width(columns)
    row = lax.broadcasted_iota(jnp.int32, (BLOCK, width), 0)
    lane = lax.broadcasted_iota(jnp.int32, (BLOCK, width), 1) % HD
    strict = lane < row
    closed = lane <= row
    eye = (lane == row).astype(F32)
    tril = (
        lax.broadcasted_iota(jnp.int32, (BLOCK, BLOCK), 1)
        <= lax.broadcasted_iota(jnp.int32, (BLOCK, BLOCK), 0)
    ).astype(F32)
    ones = head_ones(width)

    @pl.when(pl.program_id(0) == 0)
    def _():
        for group in range(columns // width):
            carry[0, group] = eye
            carry[1, group] = jnp.zeros_like(eye)

    for group in range(columns // width):
        at = pl.ds(group * width, width)
        readout = r_ref[:, at].astype(F32)
        key = k_ref[:, at].astype(F32)
        value = v_ref[:, at]
        log_decay = jax.nn.sigmoid(d_ref[:, at].astype(F32)) * -0.6065306597126334
        rate = jax.nn.sigmoid(a_ref[:, at].astype(F32))
        unit = key * lax.rsqrt(dot_exact(key * key, ones) + 1.0)
        inclusive = dot_exact(tril, log_decay)
        total = inclusive[BLOCK - 1 :]
        probe = -unit * jnp.exp(inclusive - log_decay)
        removal = unit * rate
        written = key * rate
        back = jnp.exp(-inclusive)
        tail = jnp.exp(total - inclusive)
        readout = readout * jnp.exp(inclusive)
        left = jnp.concatenate([probe, readout], axis=0)
        on_removal = dot_rows(left, spread(removal * back))
        on_write = dot_rows(left, spread(written * back))
        lower = jnp.where(strict, on_removal[:BLOCK], 0.0)
        reach = jnp.where(closed, on_removal[BLOCK:], 0.0)
        lower_write = jnp.where(strict, on_write[:BLOCK], 0.0)
        reach_write = jnp.where(closed, on_write[BLOCK:], 0.0)
        value_wide = spread(value)
        on_value = dot(jnp.concatenate([lower_write, reach_write], axis=0), value_wide)
        inverse = eye + lower
        power = dot(lower, spread(lower))
        for doubling in range(BLOCK.bit_length() - 2):
            wide = spread(power)
            if doubling < BLOCK.bit_length() - 3:
                both = dot(jnp.concatenate([inverse, power], axis=0), wide)
                inverse = inverse + both[:BLOCK]
                power = both[BLOCK:]
            else:
                inverse = inverse + dot(inverse, wide)
        solved_probe = dot(inverse, spread(probe))
        solved_values = dot(inverse, spread(on_value[:BLOCK]))
        transition = eye * jnp.exp(total) + fold(dot_cols(removal * tail, solved_probe))
        increment = fold(
            dot_cols(
                jnp.concatenate([removal * tail, written * tail], axis=0),
                jnp.concatenate([solved_values.astype(BF16), value], axis=0),
            )
        )
        read_state = readout + dot(reach, spread(solved_probe))
        local_out = dot(reach, spread(solved_values)) + on_value[BLOCK:]
        left = jnp.concatenate([read_state, transition], axis=0)
        on_map = dot(left, spread(carry[0, group]))
        on_add = dot(left, spread(carry[1, group]))
        read_ref[:, at] = on_map[:BLOCK].astype(BF16)
        local_ref[:, at] = on_add[:BLOCK] + local_out
        carry[0, group] = on_map[BLOCK:]
        carry[1, group] = on_add[BLOCK:] + increment
        total_ref[0, group] = on_map[BLOCK:].astype(BF16)
        total_ref[1, group] = (on_add[BLOCK:] + increment).astype(BF16)


def block_tables(receptance, key_in, value_in, decay_in, rate_in):
    tokens, columns = receptance.shape
    width = group_width(columns)
    groups = columns // width
    rows = pl.BlockSpec((BLOCK, columns), lambda b: (b, 0))
    return pl.pallas_call(
        tables_kernel,
        grid=(tokens // BLOCK,),
        in_specs=[rows] * 5,
        out_specs=[rows, rows, pl.BlockSpec((2, groups, HD, width), lambda b: (0, 0, 0, 0))],
        out_shape=[
            jax.ShapeDtypeStruct((tokens, columns), BF16),
            jax.ShapeDtypeStruct((tokens, columns), F32),
            jax.ShapeDtypeStruct((2, groups, HD, width), BF16),
        ],
        scratch_shapes=[pltpu.VMEM((2, groups, HD, width), F32)],
        name="tables",
    )(receptance, key_in, value_in, decay_in, rate_in)


def prefix_kernel(count, own_ref, prior_ref, outgoing, incoming, before, send_sem, recv_sem):
    me = lax.axis_index("ep")
    groups = own_ref.shape[1]
    steps = [1 << s for s in range(count.bit_length() - 1)]
    barrier = pltpu.get_barrier_semaphore()
    for step in steps:

        @pl.when(me + step < count)
        def _():
            pl.semaphore_signal(
                barrier, inc=1, device_id={"ep": me + step}, device_id_type=MESH
            )

        @pl.when(me >= step)
        def _():
            pl.semaphore_signal(
                barrier, inc=1, device_id={"ep": me - step}, device_id_type=MESH
            )

    peers = sum(
        jnp.where(me + step < count, 1, 0) + jnp.where(me >= step, 1, 0) for step in steps
    )
    pl.semaphore_wait(barrier, peers)

    width = own_ref.shape[3]
    lane = lax.broadcasted_iota(jnp.int32, (HD, width), 1) % HD
    eye = (lane == lax.broadcasted_iota(jnp.int32, (HD, width), 0)).astype(F32)
    for group in range(groups):
        before[0, group] = eye
        before[1, group] = jnp.zeros_like(eye)
    for number, step in enumerate(steps):
        last = number == len(steps) - 1
        source = own_ref if number == 0 else outgoing.at[number - 1]
        target = incoming.at[number]
        if last:
            source, target = source.at[1], target.at[1]
        copy = pltpu.make_async_remote_copy(
            src_ref=source,
            dst_ref=target,
            send_sem=send_sem.at[number],
            recv_sem=recv_sem.at[number],
            device_id={"ep": lax.rem(me + step, count)},
            device_id_type=MESH,
        )

        @pl.when(me + step < count)
        def _():
            copy.start()

        @pl.when(me >= step)
        def _():
            copy.wait_recv()
            for group in range(groups):
                left = before[0, group]
                before[1, group] += dot(left, spread(incoming[number, 1, group]))
                if not last:
                    before[0, group] = dot(left, spread(incoming[number, 0, group]))

        if not last:
            for group in range(groups):
                left = own_ref[0, group]
                outgoing[number, 0, group] = dot(left, spread(before[0, group])).astype(BF16)
                outgoing[number, 1, group] = (
                    dot(left, spread(before[1, group])) + own_ref[1, group].astype(F32)
                ).astype(BF16)

        @pl.when(me + step < count)
        def _():
            copy.wait_send()

    prior_ref[...] = before[1].astype(BF16)


def entering(total):
    count = lax.axis_size("ep")
    steps = count.bit_length() - 1
    vmem = pl.BlockSpec(memory_space=pltpu.VMEM)
    return pl.pallas_call(
        functools.partial(prefix_kernel, count),
        out_shape=jax.ShapeDtypeStruct(total.shape[1:], BF16),
        in_specs=[vmem],
        out_specs=vmem,
        scratch_shapes=[
            pltpu.VMEM((steps, *total.shape), BF16),
            pltpu.VMEM((steps, *total.shape), BF16),
            pltpu.VMEM(total.shape, F32),
            pltpu.SemaphoreType.DMA((steps,)),
            pltpu.SemaphoreType.DMA((steps,)),
        ],
        compiler_params=pltpu.CompilerParams(collective_id=0, has_side_effects=True),
        name="prefix",
    )(total)


def project_kernel(read_ref, local_ref, prior_ref, gain_ref, weight_ref, out_ref, mixed):
    groups, _, width = prior_ref.shape

    @pl.when(pl.program_id(0) == 0)
    def _():
        ones = head_ones(width)
        for group in range(groups):
            at = pl.ds(group * width, width)
            heads_out = dot(read_ref[:, at], spread(prior_ref[group])) + local_ref[:, at]
            center = heads_out - dot_exact(heads_out, ones) / HD
            variance = dot_exact(center * center, ones) / HD
            mixed[:, at] = (center * lax.rsqrt(variance + 1.0) * gain_ref[:, at]).astype(BF16)

    out_ref[...] = jnp.dot(
        mixed[...], weight_ref[...], preferred_element_type=F32
    ).astype(BF16)


def project(read, local_out, prior, norm_gain, out_weight):
    tokens, columns = read.shape
    features = out_weight.shape[1]
    tile = features // 4
    whole = pl.BlockSpec((tokens, columns), lambda n: (0, 0))
    return pl.pallas_call(
        project_kernel,
        grid=(features // tile,),
        in_specs=[
            whole,
            whole,
            pl.BlockSpec(prior.shape, lambda n: (0, 0, 0)),
            pl.BlockSpec((1, columns), lambda n: (0, 0)),
            pl.BlockSpec((columns, tile), lambda n: (0, n)),
        ],
        out_specs=pl.BlockSpec((tokens, tile), lambda n: (0, n)),
        out_shape=jax.ShapeDtypeStruct((tokens, features), BF16),
        scratch_shapes=[pltpu.VMEM((tokens, columns), BF16)],
        name="project",
    )(read, local_out, prior, norm_gain[None], out_weight)


def mixer_half(receptance, key_in, value_in, decay_in, rate_in, norm_gain, out_weight):
    read, local_out, total = block_tables(receptance, key_in, value_in, decay_in, rate_in)
    prior = entering(total)
    product = project(read, local_out, prior, norm_gain, out_weight)
    return lax.psum_scatter(product, "tp", scatter_dimension=0, tiled=True)


def hidden_kernel(rows_ref, gate_ref, up_ref, hidden_ref, gate, up):
    step = pl.program_id(0)

    @pl.when(step == 0)
    def _():
        gate[...] = jnp.zeros_like(gate)
        up[...] = jnp.zeros_like(up)

    gate[...] += jnp.dot(rows_ref[0], gate_ref[0], preferred_element_type=F32)
    up[...] += jnp.dot(rows_ref[0], up_ref[0], preferred_element_type=F32)

    @pl.when(step == pl.num_programs(0) - 1)
    def _():
        hidden_ref[...] = (jax.nn.silu(gate[...]) * up[...]).astype(BF16)


def expert_hidden(rows, gate_weight, up_weight):
    parts, row_count, part_width = rows.shape
    units = gate_weight.shape[2]
    weights = pl.BlockSpec((1, part_width, units), lambda t: (0, t, 0))
    return pl.pallas_call(
        hidden_kernel,
        grid=(parts,),
        in_specs=[
            pl.BlockSpec((1, row_count, part_width), lambda t: (t, 0, 0)),
            weights,
            weights,
        ],
        out_specs=pl.BlockSpec((row_count, units), lambda t: (0, 0)),
        out_shape=jax.ShapeDtypeStruct((row_count, units), BF16),
        scratch_shapes=[pltpu.VMEM((row_count, units), F32)] * 2,
        name="hidden",
    )(rows, gate_weight, up_weight)


def expert_half(moe_in, ffn_gain, routes, route_weights, gate_weight, up_weight, down_weight):
    row_count, feature_count = moe_in.shape
    choose_count = routes.shape[1]
    ep_count = lax.axis_size("ep")
    tp_count = lax.axis_size("tp")
    expert_count = gate_weight.shape[0] * ep_count
    capacity = 5 * row_count * choose_count // (4 * expert_count)
    part_width = feature_count // tp_count
    row_values = moe_in.astype(F32)
    scale = lax.rsqrt(jnp.mean(row_values * row_values, axis=-1, keepdims=True) + 1.0)
    first = lax.axis_index("tp") * part_width
    piece = (
        lax.dynamic_slice_in_dim(moe_in, first, part_width, 1).astype(F32)
        * scale
        * lax.dynamic_slice_in_dim(ffn_gain, first, part_width, 0)
    ).astype(BF16)
    portion = route_weights / jnp.sum(route_weights, axis=-1, keepdims=True)
    experts = jnp.arange(expert_count, dtype=jnp.int32)
    table = jnp.sum(
        jnp.where(routes[:, :, None] == experts[None, None, :], portion[:, :, None], 0.0), axis=1
    )
    high = table.astype(BF16)
    low = (table - high.astype(F32)).astype(BF16)
    extra = jnp.pad(jnp.concatenate([high, low], axis=1), ((0, 0), (0, 128 - 2 * expert_count)))
    arrived = lax.all_gather(jnp.concatenate([piece, extra], axis=1), "ep")
    mine = lax.axis_index("ep")
    shares = arrived[:, :, part_width:].astype(F32)
    shares = jnp.sum(
        jnp.where(
            lax.broadcasted_iota(jnp.int32, (1, 1, 128), 2) % expert_count == mine, shares, 0.0
        )
        * (lax.broadcasted_iota(jnp.int32, (1, 1, 128), 2) < 2 * expert_count),
        axis=-1,
    )
    named = shares > 0
    earlier = jnp.triu(jnp.ones((row_count, row_count), F32), 1)
    rank = jnp.dot(named.astype(F32), earlier)
    slots = jnp.arange(capacity, dtype=F32)
    chosen = (rank[:, None, :] == slots[None, :, None]) & named[:, None, :]
    onehot = chosen.astype(BF16)
    rows = jnp.einsum(
        "scr,srn->scn", onehot, arrived[:, :, :part_width], preferred_element_type=F32
    ).astype(BF16)
    rows = lax.all_gather(rows.reshape(ep_count * capacity, part_width), "tp")
    hidden = expert_hidden(rows, gate_weight, up_weight)
    hidden = lax.all_gather(hidden, "tp", axis=1, tiled=True)
    result = jnp.dot(hidden, down_weight[0], preferred_element_type=F32)
    slot_share = jnp.sum(jnp.where(chosen, shares[:, None, :], 0.0), axis=-1)
    result = result.reshape(ep_count, capacity, -1) * slot_share[:, :, None]
    placed = jnp.einsum(
        "scr,scd->srd", onehot, result.astype(BF16), preferred_element_type=F32
    ).astype(BF16)
    return lax.psum_scatter(
        placed.reshape(ep_count * row_count, -1), "ep", scatter_dimension=0, tiled=True
    )


def local(
    receptance,
    key_in,
    value_in,
    decay_in,
    rate_in,
    norm_gain,
    out_weight,
    moe_in,
    ffn_gain,
    routes,
    route_weights,
    gate_weight,
    up_weight,
    down_weight,
):
    mixer_out = mixer_half(receptance, key_in, value_in, decay_in, rate_in, norm_gain, out_weight)
    moe_out = expert_half(
        moe_in, ffn_gain, routes, route_weights, gate_weight, up_weight, down_weight
    )
    return (mixer_out, moe_out)


def solution(mesh):
    return jax.shard_map(
        local,
        mesh=mesh,
        in_specs=(
            P("ep", "tp"),
            P("ep", "tp"),
            P("ep", "tp"),
            P("ep", "tp"),
            P("ep", "tp"),
            P("tp"),
            P("tp", None),
            P("ep", None),
            P(),
            P("ep", None),
            P("ep", None),
            P("ep", None, "tp"),
            P("ep", None, "tp"),
            P("ep", None, "tp"),
        ),
        out_specs=(P(("ep", "tp"), None), P("ep", "tp")),
        check_vma=False,
    )
```

profile of v0, /device:TPU:0, one launch (start us, length us, event | category | flops | bytes accessed | tf_op | source)
XLA Modules:
  0.0 239.8 jit_solution(14551661261723446786)
XLA Ops:
  7.2 0.0 copy-start
  7.2 0.0 all-gather.9.cloned.1.call-start
  7.2 1.7 multiply_reduce_fusion
  8.9 0.7 reduce_sum.46
  9.6 0.7 broadcast_divide_fusion
  10.3 0.7 select_reduce_fusion.1
  11.0 0.1 copy.22
  11.1 0.7 dynamic_slice.7
  11.8 1.1 multiply_convert_fusion.1
  12.9 0.7 fusion.16
  13.6 0.0 all-gather.9.cloned.1.call-update
  13.7 0.0 all-gather.5.cloned.1.call-start
  13.7 34.3 %all-gather.9.cloned.1.call-done = bf16[1024,1152]{1,0:T(8,128)(2,1)} async-done(((bf16[128,1152]{1,0:T(8,128)(2,1)}), bf16[1024,1152]{1,0:T(8,128)(2,1)}) %all-gather.9.cloned.1.call-update) | async-done | bytes 2359312 | tf_op jit(solution)/shard_map/all_gather | solution.py:365
  48.0 1.2 multiply_reduce_fusion.1
  49.2 0.1 fusion.21
  49.3 3.2 %fusion.6 = bf16[8,80,1024]{2,1,0:T(8,128)(2,1)} fusion(bf16[8,128,1152]{2,1,0:T(8,128)(2,1)} %bitcast.17, f32[8,128]{1,0:T(8,128)S(1)} %fusion.21, pred[8,128]{1,0:T(8,128)(4,1)S(1)} %broadcast_compare_fusion), kind=kOutput, calls=%fused_computation.7 | convolution fusion | flops 168591360 | bytes 3412992 | tf_op jit(solution)/shard_map/scr,srn->scn/dot_general | solution.py:381
  52.5 0.0 all-gather.5.cloned.1.call-update
  52.5 0.0 all-gather.7.cloned.1.call-start
  52.6 60.7 %all-gather.5.cloned.1.call-done.rows_ref = bf16[4,640,1024]{2,1,0:T(8,128)(2,1)} async-done(((bf16[1,640,1024]{2,1,0:T(8,128)(2,1)}), bf16[4,640,1024]{2,1,0:T(8,128)(2,1)}) %all-gather.5.cloned.1.call-update) | async-done | bytes 5242896 | tf_op jit(solution)/shard_map/all_gather | solution.py:384
  113.2 6.9 %hidden.1 = bf16[640,256]{1,0:T(8,128)(2,1)} custom-call(bf16[4,640,1024]{2,1,0:T(8,128)(2,1)} %all-gather.5.cloned.1.call-done.rows_ref, bf16[1,4096,256]{2,1,0:T(8,128)(2,1)} %gate_ref.1, bf16[1,4096,256]{2,1,0:T(8,128)(2,1)} %up_ref.1), custom_call_target="tpu_custom_call" | custom-call | tf_op jit(solution)/shard_map/hidden/pallas_call | solution.py:326
  120.1 0.0 all-gather.7.cloned.1.call-update
  120.1 0.0 reduce-scatter.3.cloned.1.call-start
  120.2 18.1 %tables.1 = (bf16[256,512]{1,0:T(8,128)(2,1)}, f32[256,512]{1,0:T(8,128)}, bf16[2,2,64,256]{3,2,1,0:T(8,128)(2,1)}) custom-call(bf16[256,512]{1,0:T(8,128)(2,1)} %r_ref.1, bf16[256,512]{1,0:T(8,128)(2,1)} %k_ref.1, bf16[256,512]{1,0:T(8,128)(2,1)} %v_ref.1, bf16[256,512]{1,0:T(8,128)(2,1)} %d_ref.1, bf16[256,512]{1,0:T(8,128)(2,1)} %a_ref.1), custom_call_target="tpu_custom_call" | custom-call | tf_op jit(solution)/shard_map/tables/pallas_call | solution.py:150
  138.3 10.9 %prefix.1.prior_ref = bf16[2,64,256]{2,1,0:T(8,128)(2,1)} custom-call(bf16[2,2,64,256]{3,2,1,0:T(8,128)(2,1)} %get-tuple-element.7.own_ref), custom_call_target="tpu_custom_call" | custom-call | tf_op jit(solution)/shard_map/prefix/pallas_call | solution.py:242
  149.2 7.3 %project.1 = bf16[256,4096]{1,0:T(8,128)(2,1)} custom-call(bf16[256,512]{1,0:T(8,128)(2,1)} %get-tuple-element.5.read_ref, f32[256,512]{1,0:T(8,128)} %get-tuple-element.6.local_ref, bf16[2,64,256]{2,1,0:T(8,128)(2,1)} %prefix.1.prior_ref, f32[1,512]{1,0:T(1,128)} %bitcast.19, bf16[512,4096]{1,0:T(8,128)(2,1)} %weight_ref.1), custom_call_target="tpu_custom_call" | custom-call | tf_op jit(solution)/shard_map/project/pallas_call | solution.py:282
  156.5 0.0 reduce-scatter.3.cloned.1.call-update
  156.5 0.0 reduce-scatter.5.cloned.1.call-start
  156.6 0.2 select_reduce_fusion
  156.8 0.0 all-gather.7.cloned.1.call-done
  156.8 0.0 copy-done
  156.9 4.7 %convolution_convert_fusion = bf16[8,128,1024]{2,1,0:T(8,128)(2,1)} fusion(bf16[8,80,1024]{2,1,0:T(8,128)(2,1)} %bitcast.20, bf16[1,1024,1024]{2,1,0:T(8,128)(2,1)S(1)} %copy-done, f32[8,80]{1,0:T(8,128)S(1)} %select_reduce_fusion, f32[8,128]{1,0:T(8,128)S(1)} %fusion.21, pred[8,128]{1,0:T(8,128)(4,1)S(1)} %broadcast_compare_fusion), kind=kOutput, calls=%fused_computation.6 | convolution fusion | flops 1512472576 | bytes 5512704 | tf_op jit(solution)/shard_map/scr,scd->srd/dot_general | solution.py:390
  161.5 0.0 reduce-scatter.5.cloned.1.call-update
  161.6 32.9 %reduce-scatter.3.cloned.1.call-done = bf16[64,4096]{1,0:T(8,128)(2,1)} async-done(((bf16[256,4096]{1,0:T(8,128)(2,1)}), bf16[64,4096]{1,0:T(8,128)(2,1)}) %reduce-scatter.3.cloned.1.call-update) | async-done | bytes 524304 | tf_op jit(solution)/shard_map/reduce_scatter | solution.py:303
  194.5 38.8 %reduce-scatter.5.cloned.1.call-done = bf16[128,1024]{1,0:T(8,128)(2,1)} async-done(((bf16[1024,1024]{1,0:T(8,128)(2,1)}), bf16[128,1024]{1,0:T(8,128)(2,1)}) %reduce-scatter.5.cloned.1.call-update) | async-done | bytes 262160 | tf_op jit(solution)/shard_map/reduce_scatter | solution.py:393
  (5 shorter events, 0.0 us)
Async XLA Ops:
  7.2 149.7 %copy-start = (bf16[1,1024,1024]{2,1,0:T(8,128)(2,1)S(1)}, bf16[1,1024,1024]{2,1,0:T(8,128)(2,1)}, u32[]{:S(2)}) copy-start(bf16[1,1024,1024]{2,1,0:T(8,128)(2,1)} %param.27) | copy-start | bytes 6291460
  7.2 40.8 %all-gather.9.cloned.1.call-start = ((), (), s32[]{:S(2)}) async-start(), calls=%async_computation.6 | async-start | bytes 2654208 | tf_op jit(solution)/shard_map/all_gather | solution.py:365
  13.7 99.5 %all-gather.5.cloned.1.call-start = ((), (), s32[]{:S(2)}) async-start(), calls=%async_computation.3 | async-start | bytes 6553600 | tf_op jit(solution)/shard_map/all_gather | solution.py:384
  52.5 104.3 %all-gather.7.cloned.1.call-start = ((), (), s32[]{:S(2)}) async-start(), calls=%async_computation.4 | async-start | bytes 1638400 | tf_op jit(solution)/shard_map/all_gather | solution.py:386
  120.1 74.3 %reduce-scatter.3.cloned.1.call-start = ((), (), s32[]{:S(2)}) async-start(), calls=%async_computation.2 | async-start | bytes 2621440 | tf_op jit(solution)/shard_map/reduce_scatter | solution.py:303
  156.5 76.7 %reduce-scatter.5.cloned.1.call-start = ((), (), s32[]{:S(2)}) async-start(), calls=%async_computation.5 | async-start | bytes 2359296 | tf_op jit(solution)/shard_map/reduce_scatter | solution.py:393
Sparse Core Ops, SparseCore 0:
  13.8 34.1 all-gather.8
  52.6 60.5 all-gather.4
  120.2 28.6 all-gather.6
  156.7 37.7 reduce-scatter.2
  197.2 36.0 reduce-scatter.4
where the time goes:
time: 240 us
  waiting for transfers between devices  167 us (70%)
  Pallas kernels  43.2 us (18%)
  between operations  13.9 us (6%)
  matrix products  7.99 us (3%)
  other arithmetic  6.97 us (3%)
    all_gather x1, waiting for transfers between devices, expert_half(): rows = lax.all_gather(rows.reshape(ep_count * capacity, part_width), 'tp')  60.7 us
    reduce_scatter x1, waiting for transfers between devices, expert_half(): lax.psum_scatter(placed.reshape(ep_count * row_count, -1), 'ep', scatter_...  38.8 us
    all_gather x1, waiting for transfers between devices, expert_half(): arrived = lax.all_gather(jnp.concatenate([piece, extra], axis=1), 'ep')  34.3 us
    reduce_scatter x1, waiting for transfers between devices, mixer_half(): return lax.psum_scatter(product, 'tp', scatter_dimension=0, tiled=True)  32.9 us
    pallas_call x1, Pallas kernels, block_tables(): pl.pallas_call(tables_kernel, grid=(tokens // BLOCK,), in_specs=[rows] *...  18.1 us
    pallas_call x1, Pallas kernels, entering(): pl.pallas_call(functools.partial(prefix_kernel, count), out_shape=jax.Sha...  10.9 us
    pallas_call x1, Pallas kernels, project(): pl.pallas_call(project_kernel, grid=(features // tile,), in_specs=[whole,...  7.34 us
    pallas_call x1, Pallas kernels, expert_hidden(): pl.pallas_call(hidden_kernel, grid=(parts,), in_specs=[pl.BlockSpec((1, r...  6.88 us
  transfers between devices with their start and end apart: 5, of which 4 were waited for; matrix products, arithmetic and copies ran while one was open for 2% of the time, Pallas kernels for 15%

commit v1 on v0

--- a/solution.py
+++ b/solution.py
@@ -296,10 +296,7 @@
     )(read, local_out, prior, norm_gain[None], out_weight)
 
 
-def mixer_half(receptance, key_in, value_in, decay_in, rate_in, norm_gain, out_weight):
-    read, local_out, total = block_tables(receptance, key_in, value_in, decay_in, rate_in)
-    prior = entering(total)
-    product = project(read, local_out, prior, norm_gain, out_weight)
+def scatter(product):
     return lax.psum_scatter(product, "tp", scatter_dimension=0, tiled=True)
 
 
@@ -338,7 +335,137 @@
     )(rows, gate_weight, up_weight)
 
 
-def expert_half(moe_in, ffn_gain, routes, route_weights, gate_weight, up_weight, down_weight):
+def return_kernel(count, placed_ref, out_ref, pair_in, held, from_left, from_right, sems):
+    me = lax.axis_index("ep")
+    chips = count // 2
+    core = lax.rem(me, 2)
+    chip = me // 2
+    partner = me + 1 - 2 * core
+    barrier = pltpu.get_barrier_semaphore()
+
+    def signal(to):
+        pl.semaphore_signal(barrier, inc=1, device_id={"ep": to}, device_id_type=MESH)
+
+    signal(partner)
+    pl.when(chip > 0)(lambda: signal(me - 2))
+    pl.when(chip < chips - 1)(lambda: signal(me + 2))
+    pl.semaphore_wait(
+        barrier, 1 + jnp.where(chip > 0, 1, 0) + jnp.where(chip < chips - 1, 1, 0)
+    )
+
+    def send(source, target, kind, slot, to):
+        return pltpu.make_async_remote_copy(
+            src_ref=source,
+            dst_ref=target,
+            send_sem=sems.at[kind, 0, slot],
+            recv_sem=sems.at[kind, 1, slot],
+            device_id={"ep": to},
+            device_id_type=MESH,
+        )
+
+    order = []
+    for step in range(chips):
+        order += [at for at in (chips - 1 - step, step) if at not in order]
+    pairs = [
+        send(placed_ref.at[2 * at + 1 - core], pair_in.at[at], 0, at, partner)
+        for at in range(chips)
+    ]
+    rights = [
+        send(from_left.at[at], from_left.at[at], 1, at, jnp.minimum(me + 2, count - 2 + core))
+        for at in range(chips)
+    ]
+    lefts = [
+        send(from_right.at[at], from_right.at[at], 2, at, jnp.maximum(me - 2, core))
+        for at in range(chips)
+    ]
+    first_rights = [
+        send(held.at[at], from_left.at[at], 1, at, jnp.minimum(me + 2, count - 2 + core))
+        for at in range(chips)
+    ]
+    first_lefts = [
+        send(held.at[at], from_right.at[at], 2, at, jnp.maximum(me - 2, core))
+        for at in range(chips)
+    ]
+    for at in order:
+        pairs[at].start()
+
+    def pair_sum(at):
+        pairs[at].wait_recv()
+        held[at] = (
+            placed_ref[2 * at + core].astype(F32) + pair_in[at].astype(F32)
+        ).astype(BF16)
+
+    def forward(at, moving, first, relay, landing, origin):
+        @pl.when(moving & origin)
+        def _():
+            first.start()
+
+        @pl.when(moving & jnp.logical_not(origin))
+        def _():
+            relay.wait_recv()
+            landing[at] = (landing[at].astype(F32) + held[at].astype(F32)).astype(BF16)
+            relay.start()
+
+    ready = []
+    for step in range(chips):
+        for at in (chips - 1 - step, step):
+            if at not in ready:
+                pair_sum(at)
+                ready.append(at)
+        at = chips - 1 - step
+        if at > 0:
+            forward(at, at > chip, first_rights[at], rights[at], from_left, chip == 0)
+        at = step
+        if at < chips - 1:
+            forward(at, at < chip, first_lefts[at], lefts[at], from_right, chip == chips - 1)
+    out_ref[...] = held[chip]
+
+    for at in range(chips):
+
+        @pl.when((at == chip) & (chip > 0))
+        def _():
+            rights[at].wait_recv()
+            out_ref[...] = (out_ref[...].astype(F32) + from_left[at].astype(F32)).astype(BF16)
+
+        @pl.when((at == chip) & (chip < chips - 1))
+        def _():
+            lefts[at].wait_recv()
+            out_ref[...] = (out_ref[...].astype(F32) + from_right[at].astype(F32)).astype(BF16)
+
+    for at in range(chips):
+        pairs[at].wait_send()
+        pl.when(at > chip)(rights[at].wait_send)
+        pl.when(at < chip)(lefts[at].wait_send)
+
+
+def returned(placed):
+    count, rows, width = placed.shape
+    chips = count // 2
+    vmem = pl.BlockSpec(memory_space=pltpu.VMEM)
+    return pl.pallas_call(
+        functools.partial(return_kernel, count),
+        out_shape=jax.ShapeDtypeStruct((rows, width), BF16),
+        in_specs=[vmem],
+        out_specs=vmem,
+        scratch_shapes=[pltpu.VMEM((chips, rows, width), BF16)] * 4
+        + [pltpu.SemaphoreType.DMA((3, 2, chips))],
+        compiler_params=pltpu.CompilerParams(collective_id=1, has_side_effects=True),
+        name="return",
+    )(placed)
+
+
+def both_halves(
+    mixer_args,
+    norm_gain,
+    out_weight,
+    moe_in,
+    ffn_gain,
+    routes,
+    route_weights,
+    gate_weight,
+    up_weight,
+    down_weight,
+):
     row_count, feature_count = moe_in.shape
     choose_count = routes.shape[1]
     ep_count = lax.axis_size("ep")
@@ -363,6 +490,8 @@
     low = (table - high.astype(F32)).astype(BF16)
     extra = jnp.pad(jnp.concatenate([high, low], axis=1), ((0, 0), (0, 128 - 2 * expert_count)))
     arrived = lax.all_gather(jnp.concatenate([piece, extra], axis=1), "ep")
+    tables = block_tables(*mixer_args)
+    arrived, (read, local_out, total) = lax.optimization_barrier((arrived, tables))
     mine = lax.axis_index("ep")
     shares = arrived[:, :, part_width:].astype(F32)
     shares = jnp.sum(
@@ -382,17 +511,19 @@
         "scr,srn->scn", onehot, arrived[:, :, :part_width], preferred_element_type=F32
     ).astype(BF16)
     rows = lax.all_gather(rows.reshape(ep_count * capacity, part_width), "tp")
+    prior = entering(total)
+    product = project(read, local_out, prior, norm_gain, out_weight)
+    rows, product = lax.optimization_barrier((rows, product))
     hidden = expert_hidden(rows, gate_weight, up_weight)
     hidden = lax.all_gather(hidden, "tp", axis=1, tiled=True)
+    hidden, product = lax.optimization_barrier((hidden, product))
     result = jnp.dot(hidden, down_weight[0], preferred_element_type=F32)
     slot_share = jnp.sum(jnp.where(chosen, shares[:, None, :], 0.0), axis=-1)
     result = result.reshape(ep_count, capacity, -1) * slot_share[:, :, None]
     placed = jnp.einsum(
         "scr,scd->srd", onehot, result.astype(BF16), preferred_element_type=F32
     ).astype(BF16)
-    return lax.psum_scatter(
-        placed.reshape(ep_count * row_count, -1), "ep", scatter_dimension=0, tiled=True
-    )
+    return scatter(product), returned(placed)
 
 
 def local(
@@ -411,11 +542,18 @@
     up_weight,
     down_weight,
 ):
-    mixer_out = mixer_half(receptance, key_in, value_in, decay_in, rate_in, norm_gain, out_weight)
-    moe_out = expert_half(
-        moe_in, ffn_gain, routes, route_weights, gate_weight, up_weight, down_weight
-    )
-    return (mixer_out, moe_out)
+    return both_halves(
+        (receptance, key_in, value_in, decay_in, rate_in),
+        norm_gain,
+        out_weight,
+        moe_in,
+        ffn_gain,
+        routes,
+        route_weights,
+        gate_weight,
+        up_weight,
+        down_weight,
+    )
 
 
 def solution(mesh):

time: 240 us -> 199 us (0.83)
  waiting for transfers between devices: 167 us -> 88.3 us
  Pallas kernels: 43.2 us -> 78.6 us
  local copies, waits for them, and re-layouts: 0.82 us -> 3.55 us
    reduce_scatter x2 -> x1, waiting for transfers between devices: 71.7 us -> 0.02 us  [scatter(): return lax.psum_scatter(product, 'tp', scatter_dimension=0, tiled=True)]
    pallas_call x0 -> x1, Pallas kernels: none -> 36.1 us  [returned(): pl.pallas_call(functools.partial(return_kernel, count), out_shape=jax.Sha...]
    all_gather x3, waiting for transfers between devices: 94.9 us -> 88.2 us  [the longest x1 43.2 us: both_halves(): rows = lax.all_gather(rows.reshape(ep_count * capacity, part_width), 'tp')]
    unnamed x3 -> x6, local copies, waits for them, and re-layouts: 0.13 us -> 2.86 us
  transfers between devices with their start and end apart: 5 -> 4, of which waited for: 4 -> 3; matrix products, arithmetic and copies ran while one was open for 2% -> 2% of each run, Pallas kernels for 15% -> 36%
where the time goes in v1:
time: 199 us; the launch traced here: 198 us
  waiting for transfers between devices  88.3 us (44%)
  Pallas kernels  78.6 us (39%)
  between operations  13.9 us (7%)
  other arithmetic  6.98 us (4%)
  matrix products  6.74 us (3%)
  local copies, waits for them, and re-layouts  3.55 us (2%)
    all_gather x1, waiting for transfers between devices, both_halves(): rows = lax.all_gather(rows.reshape(ep_count * capacity, part_width), 'tp')  43.2 us
    pallas_call x1, Pallas kernels, returned(): pl.pallas_call(functools.partial(return_kernel, count), out_shape=jax.Sha...  36.1 us
    all_gather x1, waiting for transfers between devices, both_halves(): hidden = lax.all_gather(hidden, 'tp', axis=1, tiled=True)  28.6 us
    pallas_call x1, Pallas kernels, block_tables(): pl.pallas_call(tables_kernel, grid=(tokens // BLOCK,), in_specs=[rows] *...  18.1 us
    all_gather x1, waiting for transfers between devices, both_halves(): arrived = lax.all_gather(jnp.concatenate([piece, extra], axis=1), 'ep')  16.4 us
    pallas_call x1, Pallas kernels, entering(): pl.pallas_call(functools.partial(prefix_kernel, count), out_shape=jax.Sha...  10.1 us
    pallas_call x1, Pallas kernels, project(): pl.pallas_call(project_kernel, grid=(features // tile,), in_specs=[whole,...  7.37 us
    pallas_call x1, Pallas kernels, expert_hidden(): pl.pallas_call(hidden_kernel, grid=(parts,), in_specs=[pl.BlockSpec((1, r...  6.85 us
  transfers between devices with their start and end apart: 4, of which 3 were waited for; matrix products, arithmetic and copies ran while one was open for 2% of the time, Pallas kernels for 36%

profile of v1, /device:TPU:0, one launch (start us, length us, event | category | flops | bytes accessed | tf_op | source)
XLA Modules:
  0.0 198.2 jit_solution(8574156546401352599)
XLA Ops:
  7.2 0.0 copy-start
  7.2 0.0 all-gather.9.cloned.1.call-start
  7.2 1.7 multiply_reduce_fusion
  8.9 0.7 reduce_sum.46
  9.6 0.7 broadcast_divide_fusion
  10.3 0.7 select_reduce_fusion.1
  11.0 0.1 copy.22
  11.1 0.7 dynamic_slice.7
  11.8 1.1 multiply_convert_fusion.1
  12.9 0.7 fusion.16
  13.6 0.0 all-gather.9.cloned.1.call-update
  13.7 0.0 all-gather.5.cloned.1.call-start
  13.7 18.1 %tables.1 = (bf16[256,512]{1,0:T(8,128)(2,1)}, f32[256,512]{1,0:T(8,128)}, bf16[2,2,64,256]{3,2,1,0:T(8,128)(2,1)}) custom-call(bf16[256,512]{1,0:T(8,128)(2,1)} %r_ref.1, bf16[256,512]{1,0:T(8,128)(2,1)} %k_ref.1, bf16[256,512]{1,0:T(8,128)(2,1)} %v_ref.1, bf16[256,512]{1,0:T(8,128)(2,1)} %d_ref.1, bf16[256,512]{1,0:T(8,128)(2,1)} %a_ref.1), custom_call_target="tpu_custom_call" | custom-call | tf_op jit(solution)/shard_map/tables/pallas_call | solution.py:150
  31.8 16.4 %all-gather.9.cloned.1.call-done = bf16[1024,1152]{1,0:T(8,128)(2,1)} async-done(((bf16[128,1152]{1,0:T(8,128)(2,1)}), bf16[1024,1152]{1,0:T(8,128)(2,1)}) %all-gather.9.cloned.1.call-update) | async-done | bytes 2359312 | tf_op jit(solution)/shard_map/all_gather | solution.py:492
  48.2 1.2 multiply_reduce_fusion.1
  49.4 0.1 fusion.21
  49.5 3.2 %fusion.4 = bf16[8,80,1024]{2,1,0:T(8,128)(2,1)} fusion(bf16[8,128,1152]{2,1,0:T(8,128)(2,1)} %bitcast.16, f32[8,128]{1,0:T(8,128)S(1)} %fusion.21, pred[8,128]{1,0:T(8,128)(4,1)S(1)} %broadcast_compare_fusion), kind=kOutput, calls=%fused_computation.7 | convolution fusion | flops 168591360 | bytes 3412992 | tf_op jit(solution)/shard_map/scr,srn->scn/dot_general | solution.py:510
  52.7 0.0 all-gather.5.cloned.1.call-update
  52.7 0.0 all-gather.7.cloned.1.call-start
  52.8 10.1 %prefix.1.prior_ref = bf16[2,64,256]{2,1,0:T(8,128)(2,1)} custom-call(bf16[2,2,64,256]{3,2,1,0:T(8,128)(2,1)} %get-tuple-element.19.own_ref), custom_call_target="tpu_custom_call" | custom-call | tf_op jit(solution)/shard_map/prefix/pallas_call | solution.py:242
  63.0 7.4 %project.1 = bf16[256,4096]{1,0:T(8,128)(2,1)} custom-call(bf16[256,512]{1,0:T(8,128)(2,1)} %get-tuple-element.17.read_ref, f32[256,512]{1,0:T(8,128)} %get-tuple-element.18.local_ref, bf16[2,64,256]{2,1,0:T(8,128)(2,1)} %prefix.1.prior_ref, f32[1,512]{1,0:T(1,128)} %bitcast.17, bf16[512,4096]{1,0:T(8,128)(2,1)} %weight_ref.1), custom_call_target="tpu_custom_call" | custom-call | tf_op jit(solution)/shard_map/project/pallas_call | solution.py:282
  70.3 43.2 %all-gather.5.cloned.1.call-done.rows_ref = bf16[4,640,1024]{2,1,0:T(8,128)(2,1)} async-done(((bf16[1,640,1024]{2,1,0:T(8,128)(2,1)}), bf16[4,640,1024]{2,1,0:T(8,128)(2,1)}) %all-gather.5.cloned.1.call-update) | async-done | bytes 5242896 | tf_op jit(solution)/shard_map/all_gather | solution.py:513
  113.5 6.8 %hidden.1 = bf16[640,256]{1,0:T(8,128)(2,1)} custom-call(bf16[4,640,1024]{2,1,0:T(8,128)(2,1)} %all-gather.5.cloned.1.call-done.rows_ref, bf16[1,4096,256]{2,1,0:T(8,128)(2,1)} %gate_ref.1, bf16[1,4096,256]{2,1,0:T(8,128)(2,1)} %up_ref.1), custom_call_target="tpu_custom_call" | custom-call | tf_op jit(solution)/shard_map/hidden/pallas_call | solution.py:323
  120.3 0.0 all-gather.7.cloned.1.call-update
  120.4 0.0 reduce-scatter.2.cloned.1.call-start
  120.4 28.6 %all-gather.7.cloned.1.call-done = bf16[640,1024]{1,0:T(8,128)(2,1)} async-done(((bf16[640,256]{1,0:T(8,128)(2,1)}), bf16[640,1024]{1,0:T(8,128)(2,1)}) %all-gather.7.cloned.1.call-update) | async-done | bytes 1310736 | tf_op jit(solution)/shard_map/all_gather | solution.py:518
  149.1 0.0 copy-start.1
  149.1 0.0 reduce-scatter.2.cloned.1.call-update
  149.1 0.2 select_reduce_fusion
  149.3 0.0 copy-done
  149.3 1.1 copy-done.1
  150.4 3.4 %convolution_convert_fusion.placed_ref = bf16[8,128,1024]{2,1,0:T(8,128)(2,1)} fusion(bf16[8,80,1024]{2,1,0:T(8,128)(2,1)S(1)} %bitcast.18, bf16[1,1024,1024]{2,1,0:T(8,128)(2,1)S(1)} %copy-done, f32[8,80]{1,0:T(8,128)S(1)} %select_reduce_fusion, f32[8,128]{1,0:T(8,128)S(1)} %fusion.21, pred[8,128]{1,0:T(8,128)(4,1)S(1)} %broadcast_compare_fusion), kind=kOutput, calls=%fused_computation.6 | convolution fusion | flops 1512472576 | bytes 5512704 | tf_op jit(solution)/shard_map/scr,scd->srd/dot_general | solution.py:523
  153.8 36.1 %return.1 = bf16[128,1024]{1,0:T(8,128)(2,1)} custom-call(bf16[8,128,1024]{2,1,0:T(8,128)(2,1)} %convolution_convert_fusion.placed_ref), custom_call_target="tpu_custom_call" | custom-call | tf_op jit(solution)/shard_map/return/pallas_call | solution.py:445
  189.9 0.0 reduce-scatter.2.cloned.1.call-done
  190.0 1.7 copy.24
  (5 shorter events, 0.0 us)
Async XLA Ops:
  7.2 142.2 %copy-start = (bf16[1,1024,1024]{2,1,0:T(8,128)(2,1)S(1)}, bf16[1,1024,1024]{2,1,0:T(8,128)(2,1)}, u32[]{:S(2)}) copy-start(bf16[1,1024,1024]{2,1,0:T(8,128)(2,1)} %param.27) | copy-start | bytes 6291460
  7.2 41.0 %all-gather.9.cloned.1.call-start = ((), (), s32[]{:S(2)}) async-start(), calls=%async_computation.4 | async-start | bytes 2654208 | tf_op jit(solution)/shard_map/all_gather | solution.py:492
  13.7 99.8 %all-gather.5.cloned.1.call-start = ((), (), s32[]{:S(2)}) async-start(), calls=%async_computation.1 | async-start | bytes 6553600 | tf_op jit(solution)/shard_map/all_gather | solution.py:513
  52.7 96.3 %all-gather.7.cloned.1.call-start = ((), (), s32[]{:S(2)}) async-start(), calls=%async_computation.2 | async-start | bytes 1638400 | tf_op jit(solution)/shard_map/all_gather | solution.py:518
  120.4 69.6 %reduce-scatter.2.cloned.1.call-start = ((), (), s32[]{:S(2)}) async-start(), calls=%async_computation.3 | async-start | bytes 2621440 | tf_op jit(solution)/shard_map/reduce_scatter | solution.py:300
  149.1 1.3 copy-start.1
Sparse Core Ops, SparseCore 0:
  13.8 34.3 all-gather.8
  52.9 60.5 all-gather.4
  120.5 28.5 all-gather.6
  152.5 35.1 reduce-scatter.1

commit v2 on v1

--- a/solution.py
+++ b/solution.py
@@ -162,30 +162,71 @@
     )(receptance, key_in, value_in, decay_in, rate_in)
 
 
-def prefix_kernel(count, own_ref, prior_ref, outgoing, incoming, before, send_sem, recv_sem):
+def flip(me, bits):
+    bit = 1
+    while bit <= bits:
+        if bits & bit:
+            me = me + bit - 2 * bit * ((me // bit) % 2)
+        bit *= 2
+    return me
+
+
+class Exchange:
+    def __init__(self, count, own, slots, sems):
+        me = lax.axis_index("tp")
+        half = own.shape[0] // 2
+        bits = [1 << b for b in range(count.bit_length() - 1)]
+        self.count, self.copies, self.heads, self.relays, self.seen = count, {}, [], [], set()
+        for number in range(len(bits)):
+            for stream, order in enumerate((bits, bits[::-1])):
+                at = pl.ds(stream * half, half)
+                known = [0]
+                for bit in order[:number]:
+                    known += [k ^ bit for k in known]
+                for from_delta in known:
+                    bit = order[number]
+                    key = (stream, from_delta ^ bit)
+                    owner = flip(me, from_delta)
+                    self.copies[key] = pltpu.make_async_remote_copy(
+                        src_ref=slots.at[owner, at] if from_delta else own.at[at],
+                        dst_ref=slots.at[owner, at],
+                        send_sem=sems.at[0, stream, key[1]],
+                        recv_sem=sems.at[1, stream, key[1]],
+                        device_id={"tp": flip(me, bit)},
+                        device_id_type=MESH,
+                    )
+                    if from_delta:
+                        self.relays.append((key, from_delta))
+                    else:
+                        self.heads.append(key)
+
+    def start(self):
+        for key in self.heads:
+            self.copies[key].start()
+
+    def arrive(self, stream, delta):
+        if (stream, delta) not in self.seen:
+            self.seen.add((stream, delta))
+            self.copies[stream, delta].wait_recv()
+
+    def relay(self):
+        for key, from_delta in self.relays:
+            self.arrive(key[0], from_delta)
+            self.copies[key].start()
+
+    def wait(self, delta):
+        for stream in (0, 1):
+            self.arrive(stream, delta)
+
+    def finish(self):
+        for copy in self.copies.values():
+            copy.wait_send()
+
+
+def prefix(count, own_ref, outgoing, incoming, before, send_sem, recv_sem):
     me = lax.axis_index("ep")
     groups = own_ref.shape[1]
     steps = [1 << s for s in range(count.bit_length() - 1)]
-    barrier = pltpu.get_barrier_semaphore()
-    for step in steps:
-
-        @pl.when(me + step < count)
-        def _():
-            pl.semaphore_signal(
-                barrier, inc=1, device_id={"ep": me + step}, device_id_type=MESH
-            )
-
-        @pl.when(me >= step)
-        def _():
-            pl.semaphore_signal(
-                barrier, inc=1, device_id={"ep": me - step}, device_id_type=MESH
-            )
-
-    peers = sum(
-        jnp.where(me + step < count, 1, 0) + jnp.where(me >= step, 1, 0) for step in steps
-    )
-    pl.semaphore_wait(barrier, peers)
-
     width = own_ref.shape[3]
     lane = lax.broadcasted_iota(jnp.int32, (HD, width), 1) % HD
     eye = (lane == lax.broadcasted_iota(jnp.int32, (HD, width), 0)).astype(F32)
@@ -232,107 +273,171 @@
         def _():
             copy.wait_send()
 
-    prior_ref[...] = before[1].astype(BF16)
-
-
-def entering(total):
-    count = lax.axis_size("ep")
-    steps = count.bit_length() - 1
+
+def experts_kernel(
+    tp_count,
+    ep_count,
+    rows_ref,
+    gate_hbm,
+    up_hbm,
+    down_hbm,
+    share_ref,
+    total_ref,
+    read_ref,
+    local_ref,
+    gain_ref,
+    weight_hbm,
+    product_ref,
+    result_ref,
+    slots,
+    hidden_slots,
+    hidden,
+    gate_w,
+    up_w,
+    down_w,
+    out_w,
+    gate,
+    up,
+    down,
+    mixed,
+    outgoing,
+    incoming,
+    before,
+    send_sem,
+    recv_sem,
+    row_sems,
+    hidden_sems,
+    load_sems,
+):
+    me = lax.axis_index("tp")
+    place = lax.axis_index("ep")
+    steps = [1 << s for s in range(ep_count.bit_length() - 1)]
+    bits = [1 << b for b in range(tp_count.bit_length() - 1)]
+    loads = [
+        pltpu.make_async_copy(source, target, load_sems.at[i])
+        for i, (source, target) in enumerate(
+            ((gate_hbm, gate_w), (up_hbm, up_w), (down_hbm, down_w), (weight_hbm, out_w))
+        )
+    ]
+    for load in loads:
+        load.start()
+    barrier = pltpu.get_barrier_semaphore()
+
+    def signal(axis, to):
+        pl.semaphore_signal(barrier, inc=1, device_id={axis: to}, device_id_type=MESH)
+
+    for bit in bits:
+        signal("tp", flip(me, bit))
+    for step in steps:
+        pl.when(place + step < ep_count)(lambda: signal("ep", place + step))
+        pl.when(place >= step)(lambda: signal("ep", place - step))
+    peers = sum(
+        jnp.where(place + step < ep_count, 1, 0) + jnp.where(place >= step, 1, 0)
+        for step in steps
+    )
+    pl.semaphore_wait(barrier, peers + len(bits))
+
+    exchange = Exchange(tp_count, rows_ref, slots, row_sems)
+    exchange.start()
+    prefix(ep_count, total_ref, outgoing, incoming, before, send_sem, recv_sem)
+    part_width = rows_ref.shape[1]
+    units = gate.shape[1]
+
+    def slice_product(block, owner, first):
+        at = pl.ds(pl.multiple_of(owner * part_width, part_width), part_width)
+        for total, weight in ((gate, gate_w), (up, up_w)):
+            product = jnp.dot(block, weight[at, :], preferred_element_type=F32)
+            total[...] = product if first else total[...] + product
+
+    loads[0].wait()
+    loads[1].wait()
+    exchange.relay()
+    slice_product(rows_ref[...], me, True)
+    columns = read_ref.shape[1]
+    groups, width = total_ref.shape[1], total_ref.shape[3]
+    ones = head_ones(width)
+    for group in range(groups):
+        at = pl.ds(group * width, width)
+        heads_out = dot(read_ref[:, at], spread(before[1, group])) + local_ref[:, at]
+        center = heads_out - dot_exact(heads_out, ones) / HD
+        variance = dot_exact(center * center, ones) / HD
+        mixed[:, at] = (center * lax.rsqrt(variance + 1.0) * gain_ref[:, at]).astype(BF16)
+    for delta in range(1, tp_count):
+        exchange.wait(delta)
+        slice_product(slots[flip(me, delta)], flip(me, delta), False)
+    hidden[...] = (jax.nn.silu(gate[...]) * up[...]).astype(BF16)
+    hidden_exchange = Exchange(tp_count, hidden, hidden_slots, hidden_sems)
+    hidden_exchange.start()
+
+    def down_product(block, owner):
+        at = pl.ds(pl.multiple_of(owner * units, units), units)
+        return jnp.dot(block, down_w[at, :], preferred_element_type=F32)
+
+    loads[2].wait()
+    loads[3].wait()
+    down[...] = down_product(hidden[...], me)
+    tile = product_ref.shape[1] // 4
+    for number in range(4):
+        at = pl.ds(number * tile, tile)
+        product_ref[:, at] = jnp.dot(
+            mixed[...], out_w[:, at], preferred_element_type=F32
+        ).astype(BF16)
+        if number == 1:
+            hidden_exchange.relay()
+    for delta in range(1, tp_count):
+        hidden_exchange.wait(delta)
+        down[...] += down_product(hidden_slots[flip(me, delta)], flip(me, delta))
+    result_ref[...] = (down[...] * share_ref[...]).astype(BF16)
+    exchange.finish()
+    hidden_exchange.finish()
+
+
+def experts(rows, gate_w, up_w, down_w, share, total, read, local_out, gain, out_w):
+    tp_count, ep_count = lax.axis_size("tp"), lax.axis_size("ep")
+    row_count, part_width = rows.shape
+    units, out_part = gate_w.shape[1], down_w.shape[1]
+    tokens, columns = read.shape
+    steps = ep_count.bit_length() - 1
     vmem = pl.BlockSpec(memory_space=pltpu.VMEM)
+    hbm = pl.BlockSpec(memory_space=pl.ANY)
     return pl.pallas_call(
-        functools.partial(prefix_kernel, count),
-        out_shape=jax.ShapeDtypeStruct(total.shape[1:], BF16),
-        in_specs=[vmem],
-        out_specs=vmem,
+        functools.partial(experts_kernel, tp_count, ep_count),
+        out_shape=[
+            jax.ShapeDtypeStruct((tokens, out_w.shape[1]), BF16),
+            jax.ShapeDtypeStruct((row_count, out_part), BF16),
+        ],
+        in_specs=[vmem, hbm, hbm, hbm, vmem, vmem, vmem, vmem, vmem, hbm],
+        out_specs=[vmem, vmem],
         scratch_shapes=[
+            pltpu.VMEM((tp_count, row_count, part_width), BF16),
+            pltpu.VMEM((tp_count, row_count, units), BF16),
+            pltpu.VMEM((row_count, units), BF16),
+            pltpu.VMEM(gate_w.shape, BF16),
+            pltpu.VMEM(up_w.shape, BF16),
+            pltpu.VMEM(down_w.shape, BF16),
+            pltpu.VMEM(out_w.shape, BF16),
+            pltpu.VMEM((row_count, units), F32),
+            pltpu.VMEM((row_count, units), F32),
+            pltpu.VMEM((row_count, out_part), F32),
+            pltpu.VMEM((tokens, columns), BF16),
             pltpu.VMEM((steps, *total.shape), BF16),
             pltpu.VMEM((steps, *total.shape), BF16),
             pltpu.VMEM(total.shape, F32),
             pltpu.SemaphoreType.DMA((steps,)),
             pltpu.SemaphoreType.DMA((steps,)),
+            pltpu.SemaphoreType.DMA((2, 2, tp_count)),
+            pltpu.SemaphoreType.DMA((2, 2, tp_count)),
+            pltpu.SemaphoreType.DMA((4,)),
         ],
-        compiler_params=pltpu.CompilerParams(collective_id=0, has_side_effects=True),
-        name="prefix",
-    )(total)
-
-
-def project_kernel(read_ref, local_ref, prior_ref, gain_ref, weight_ref, out_ref, mixed):
-    groups, _, width = prior_ref.shape
-
-    @pl.when(pl.program_id(0) == 0)
-    def _():
-        ones = head_ones(width)
-        for group in range(groups):
-            at = pl.ds(group * width, width)
-            heads_out = dot(read_ref[:, at], spread(prior_ref[group])) + local_ref[:, at]
-            center = heads_out - dot_exact(heads_out, ones) / HD
-            variance = dot_exact(center * center, ones) / HD
-            mixed[:, at] = (center * lax.rsqrt(variance + 1.0) * gain_ref[:, at]).astype(BF16)
-
-    out_ref[...] = jnp.dot(
-        mixed[...], weight_ref[...], preferred_element_type=F32
-    ).astype(BF16)
-
-
-def project(read, local_out, prior, norm_gain, out_weight):
-    tokens, columns = read.shape
-    features = out_weight.shape[1]
-    tile = features // 4
-    whole = pl.BlockSpec((tokens, columns), lambda n: (0, 0))
-    return pl.pallas_call(
-        project_kernel,
-        grid=(features // tile,),
-        in_specs=[
-            whole,
-            whole,
-            pl.BlockSpec(prior.shape, lambda n: (0, 0, 0)),
-            pl.BlockSpec((1, columns), lambda n: (0, 0)),
-            pl.BlockSpec((columns, tile), lambda n: (0, n)),
-        ],
-        out_specs=pl.BlockSpec((tokens, tile), lambda n: (0, n)),
-        out_shape=jax.ShapeDtypeStruct((tokens, features), BF16),
-        scratch_shapes=[pltpu.VMEM((tokens, columns), BF16)],
-        name="project",
-    )(read, local_out, prior, norm_gain[None], out_weight)
+        compiler_params=pltpu.CompilerParams(
+            collective_id=0, has_side_effects=True, vmem_limit_bytes=60 * 1024 * 1024
+        ),
+        name="experts",
+    )(rows, gate_w, up_w, down_w, share, total, read, local_out, gain, out_w)
 
 
 def scatter(product):
     return lax.psum_scatter(product, "tp", scatter_dimension=0, tiled=True)
-
-
-def hidden_kernel(rows_ref, gate_ref, up_ref, hidden_ref, gate, up):
-    step = pl.program_id(0)
-
-    @pl.when(step == 0)
-    def _():
-        gate[...] = jnp.zeros_like(gate)
-        up[...] = jnp.zeros_like(up)
-
-    gate[...] += jnp.dot(rows_ref[0], gate_ref[0], preferred_element_type=F32)
-    up[...] += jnp.dot(rows_ref[0], up_ref[0], preferred_element_type=F32)
-
-    @pl.when(step == pl.num_programs(0) - 1)
-    def _():
-        hidden_ref[...] = (jax.nn.silu(gate[...]) * up[...]).astype(BF16)
-
-
-def expert_hidden(rows, gate_weight, up_weight):
-    parts, row_count, part_width = rows.shape
-    units = gate_weight.shape[2]
-    weights = pl.BlockSpec((1, part_width, units), lambda t: (0, t, 0))
-    return pl.pallas_call(
-        hidden_kernel,
-        grid=(parts,),
-        in_specs=[
-            pl.BlockSpec((1, row_count, part_width), lambda t: (t, 0, 0)),
-            weights,
-            weights,
-        ],
-        out_specs=pl.BlockSpec((row_count, units), lambda t: (0, 0)),
-        out_shape=jax.ShapeDtypeStruct((row_count, units), BF16),
-        scratch_shapes=[pltpu.VMEM((row_count, units), F32)] * 2,
-        name="hidden",
-    )(rows, gate_weight, up_weight)
 
 
 def return_kernel(count, placed_ref, out_ref, pair_in, held, from_left, from_right, sems):
@@ -482,9 +587,9 @@
         * lax.dynamic_slice_in_dim(ffn_gain, first, part_width, 0)
     ).astype(BF16)
     portion = route_weights / jnp.sum(route_weights, axis=-1, keepdims=True)
-    experts = jnp.arange(expert_count, dtype=jnp.int32)
+    names = jnp.arange(expert_count, dtype=jnp.int32)
     table = jnp.sum(
-        jnp.where(routes[:, :, None] == experts[None, None, :], portion[:, :, None], 0.0), axis=1
+        jnp.where(routes[:, :, None] == names[None, None, :], portion[:, :, None], 0.0), axis=1
     )
     high = table.astype(BF16)
     low = (table - high.astype(F32)).astype(BF16)
@@ -510,18 +615,24 @@
     rows = jnp.einsum(
         "scr,srn->scn", onehot, arrived[:, :, :part_width], preferred_element_type=F32
     ).astype(BF16)
-    rows = lax.all_gather(rows.reshape(ep_count * capacity, part_width), "tp")
-    prior = entering(total)
-    product = project(read, local_out, prior, norm_gain, out_weight)
-    rows, product = lax.optimization_barrier((rows, product))
-    hidden = expert_hidden(rows, gate_weight, up_weight)
-    hidden = lax.all_gather(hidden, "tp", axis=1, tiled=True)
-    hidden, product = lax.optimization_barrier((hidden, product))
-    result = jnp.dot(hidden, down_weight[0], preferred_element_type=F32)
     slot_share = jnp.sum(jnp.where(chosen, shares[:, None, :], 0.0), axis=-1)
-    result = result.reshape(ep_count, capacity, -1) * slot_share[:, :, None]
+    product, result = experts(
+        rows.reshape(ep_count * capacity, part_width),
+        gate_weight[0],
+        up_weight[0],
+        down_weight[0],
+        slot_share.reshape(ep_count * capacity, 1),
+        total,
+        read,
+        local_out,
+        norm_gain[None],
+        out_weight,
+    )
     placed = jnp.einsum(
-        "scr,scd->srd", onehot, result.astype(BF16), preferred_element_type=F32
+        "scr,scd->srd",
+        onehot,
+        result.reshape(ep_count, capacity, -1),
+        preferred_element_type=F32,
     ).astype(BF16)
     return scatter(product), returned(placed)
 

time: 199 us -> 165 us (0.83)
  waiting for transfers between devices: 88.3 us -> 16.5 us
  Pallas kernels: 78.6 us -> 117 us
    all_gather x2 -> x0, waiting for transfers between devices: 71.8 us -> none  [the longest x1 43.2 us: both_halves(): rows = lax.all_gather(rows.reshape(ep_count * capacity, part_width), 'tp')]
    pallas_call x3 -> x1, Pallas kernels: 24.4 us -> 63.5 us  [experts(): pl.pallas_call(functools.partial(experts_kernel, tp_count, ep_count), out...]
  transfers between devices with their start and end apart: 4 -> 2, of which waited for: 3 -> 1; matrix products, arithmetic and copies ran while one was open for 2% -> 1% of each run, Pallas kernels for 36% -> 33%
where the time goes in v2:
time: 165 us
  Pallas kernels  117 us (71%)
  waiting for transfers between devices  16.5 us (10%)
  between operations  14.1 us (9%)
  other arithmetic  6.84 us (4%)
  matrix products  5.35 us (3%)
  local copies, waits for them, and re-layouts  4.65 us (3%)
    pallas_call x1, Pallas kernels, experts(): pl.pallas_call(functools.partial(experts_kernel, tp_count, ep_count), out...  63.5 us
    pallas_call x1, Pallas kernels, returned(): pl.pallas_call(functools.partial(return_kernel, count), out_shape=jax.Sha...  35.4 us
    pallas_call x1, Pallas kernels, block_tables(): pl.pallas_call(tables_kernel, grid=(tokens // BLOCK,), in_specs=[rows] *...  18.1 us
    all_gather x1, waiting for transfers between devices, both_halves(): arrived = lax.all_gather(jnp.concatenate([piece, extra], axis=1), 'ep')  16.4 us
  transfers between devices with their start and end apart: 2, of which 1 were waited for; matrix products, arithmetic and copies ran while one was open for 1% of the time, Pallas kernels for 33%

profile of v2, /device:TPU:0, one launch (start us, length us, event | category | flops | bytes accessed | tf_op | source)
XLA Modules:
  0.0 164.5 jit_solution(4237504061549317085)
XLA Ops:
  7.2 0.0 all-gather.3.cloned.1.call-start
  7.2 1.5 multiply_reduce_fusion
  8.7 0.7 reduce_sum.46
  9.4 0.7 broadcast_divide_fusion
  10.1 0.7 select_reduce_fusion.1
  10.8 0.1 copy.27
  11.0 0.7 dynamic_slice.7
  11.7 1.1 multiply_convert_fusion
  12.7 0.7 fusion.9
  13.5 0.0 all-gather.3.cloned.1.call-update
  13.5 0.0 reduce-scatter.2.cloned.1.call-start
  13.6 18.1 %tables.1 = (bf16[256,512]{1,0:T(8,128)(2,1)}, f32[256,512]{1,0:T(8,128)}, bf16[2,2,64,256]{3,2,1,0:T(8,128)(2,1)}) custom-call(bf16[256,512]{1,0:T(8,128)(2,1)} %r_ref.1, bf16[256,512]{1,0:T(8,128)(2,1)} %k_ref.1, bf16[256,512]{1,0:T(8,128)(2,1)} %v_ref.1, bf16[256,512]{1,0:T(8,128)(2,1)} %d_ref.1, bf16[256,512]{1,0:T(8,128)(2,1)} %a_ref.1), custom_call_target="tpu_custom_call" | custom-call | tf_op jit(solution)/shard_map/tables/pallas_call | solution.py:150
  31.7 16.4 %all-gather.3.cloned.1.call-done = bf16[1024,1152]{1,0:T(8,128)(2,1)} async-done(((bf16[128,1152]{1,0:T(8,128)(2,1)}), bf16[1024,1152]{1,0:T(8,128)(2,1)}) %all-gather.3.cloned.1.call-update) | async-done | bytes 2359312 | tf_op jit(solution)/shard_map/all_gather | solution.py:597
  48.1 1.2 multiply_reduce_fusion.1
  49.3 0.1 fusion.14
  49.4 3.2 %fusion.2 = bf16[8,80,1024]{2,1,0:T(8,128)(2,1)} fusion(bf16[8,128,1152]{2,1,0:T(8,128)(2,1)} %bitcast.11, f32[8,128]{1,0:T(8,128)S(1)} %fusion.14, pred[8,128]{1,0:T(8,128)(4,1)S(1)} %broadcast_compare_fusion), kind=kOutput, calls=%fused_computation.4 | convolution fusion | flops 168591360 | bytes 3412992 | tf_op jit(solution)/shard_map/scr,srn->scn/dot_general | solution.py:615
  52.6 0.2 select_reduce_fusion
  52.8 0.9 reshape.58.share_ref
  53.7 63.5 %experts.1 = (bf16[256,4096]{1,0:T(8,128)(2,1)}, bf16[640,1024]{1,0:T(8,128)(2,1)}) custom-call(bf16[640,1024]{1,0:T(8,128)(2,1)} %bitcast.9, bf16[4096,256]{1,0:T(8,128)(2,1)} %bitcast.12, bf16[4096,256]{1,0:T(8,128)(2,1)} %bitcast.13, bf16[1024,1024]{1,0:T(8,128)(2,1)} %bitcast.14, f32[640,1]{1,0:T(8,128)} %reshape.58.share_ref, ...), custom_call_target="tpu_custom_call" | custom-call | tf_op jit(solution)/shard_map/experts/pallas_call | solution.py:403
  117.2 0.0 copy-start
  117.2 0.0 reduce-scatter.2.cloned.1.call-update
  117.2 1.3 copy-done
  118.5 2.1 %convolution_convert_fusion.placed_ref = bf16[8,128,1024]{2,1,0:T(8,128)(2,1)} fusion(bf16[8,80,1024]{2,1,0:T(8,128)(2,1)S(1)} %bitcast.15, f32[8,128]{1,0:T(8,128)S(1)} %fusion.14, pred[8,128]{1,0:T(8,128)(4,1)S(1)} %broadcast_compare_fusion), kind=kOutput, calls=%fused_computation.3 | convolution fusion | flops 168984576 | bytes 3412992 | tf_op jit(solution)/shard_map/scr,scd->srd/dot_general | solution.py:631
  120.6 35.4 %return.1 = bf16[128,1024]{1,0:T(8,128)(2,1)} custom-call(bf16[8,128,1024]{2,1,0:T(8,128)(2,1)} %convolution_convert_fusion.placed_ref), custom_call_target="tpu_custom_call" | custom-call | tf_op jit(solution)/shard_map/return/pallas_call | solution.py:550
  156.0 0.0 reduce-scatter.2.cloned.1.call-done
  156.0 1.7 %copy.29 = bf16[128,1024]{1,0:T(8,128)(2,1)} copy(bf16[128,1024]{1,0:T(8,128)(2,1)} %return.1) | data formatting | bytes 524288
  (5 shorter events, 0.0 us)
Async XLA Ops:
  7.2 40.9 %all-gather.3.cloned.1.call-start = ((), (), s32[]{:S(2)}) async-start(), calls=%async_computation.2 | async-start | bytes 2654208 | tf_op jit(solution)/shard_map/all_gather | solution.py:597
  13.5 142.5 %reduce-scatter.2.cloned.1.call-start = ((), (), s32[]{:S(2)}) async-start(), calls=%async_computation.1 | async-start | bytes 2621440 | tf_op jit(solution)/shard_map/reduce_scatter | solution.py:440
  117.2 1.3 copy-start
Sparse Core Ops, SparseCore 0:
  13.6 34.3 all-gather.2
  117.4 33.8 reduce-scatter.1

commit v3 on v2

--- a/solution.py
+++ b/solution.py
@@ -458,89 +458,116 @@
         barrier, 1 + jnp.where(chip > 0, 1, 0) + jnp.where(chip < chips - 1, 1, 0)
     )
 
-    def send(source, target, kind, slot, to):
+    half = out_ref.shape[0] // 2
+    right_to = jnp.minimum(me + 2, count - 2 + core)
+    left_to = jnp.maximum(me - 2, core)
+
+    def send(source, target, kind, item, to):
+        at, part = item
+        rows = pl.ds(part * half, half)
         return pltpu.make_async_remote_copy(
-            src_ref=source,
-            dst_ref=target,
-            send_sem=sems.at[kind, 0, slot],
-            recv_sem=sems.at[kind, 1, slot],
+            src_ref=source.at[rows],
+            dst_ref=target.at[at, rows],
+            send_sem=sems.at[kind, 0, 2 * at + part],
+            recv_sem=sems.at[kind, 1, 2 * at + part],
             device_id={"ep": to},
             device_id_type=MESH,
         )
 
+    def pair(item):
+        return send(placed_ref.at[2 * item[0] + 1 - core], pair_in, 0, item, partner)
+
+    def right(item, source=from_left):
+        return send(source.at[item[0]], from_left, 1, item, right_to)
+
+    def left(item, source=from_right):
+        return send(source.at[item[0]], from_right, 2, item, left_to)
+
     order = []
     for step in range(chips):
         order += [at for at in (chips - 1 - step, step) if at not in order]
-    pairs = [
-        send(placed_ref.at[2 * at + 1 - core], pair_in.at[at], 0, at, partner)
-        for at in range(chips)
-    ]
-    rights = [
-        send(from_left.at[at], from_left.at[at], 1, at, jnp.minimum(me + 2, count - 2 + core))
-        for at in range(chips)
-    ]
-    lefts = [
-        send(from_right.at[at], from_right.at[at], 2, at, jnp.maximum(me - 2, core))
-        for at in range(chips)
-    ]
-    first_rights = [
-        send(held.at[at], from_left.at[at], 1, at, jnp.minimum(me + 2, count - 2 + core))
-        for at in range(chips)
-    ]
-    first_lefts = [
-        send(held.at[at], from_right.at[at], 2, at, jnp.maximum(me - 2, core))
-        for at in range(chips)
-    ]
-    for at in order:
-        pairs[at].start()
-
-    def pair_sum(at):
-        pairs[at].wait_recv()
-        held[at] = (
-            placed_ref[2 * at + core].astype(F32) + pair_in[at].astype(F32)
+    items = [(at, part) for at in order for part in (0, 1)]
+    for item in items:
+        pair(item).start()
+
+    def pair_sum(item):
+        at, part = item
+        rows = pl.ds(part * half, half)
+        pair(item).wait_recv()
+        held[at, rows] = (
+            placed_ref[2 * at + core, rows].astype(F32) + pair_in[at, rows].astype(F32)
         ).astype(BF16)
 
-    def forward(at, moving, first, relay, landing, origin):
+    def forward(item, moving, hop, landing, origin):
+        at, part = item
+        rows = pl.ds(part * half, half)
+
         @pl.when(moving & origin)
         def _():
-            first.start()
+            hop(item, held).start()
 
         @pl.when(moving & jnp.logical_not(origin))
         def _():
+            relay = hop(item)
             relay.wait_recv()
-            landing[at] = (landing[at].astype(F32) + held[at].astype(F32)).astype(BF16)
+            landing[at, rows] = (
+                landing[at, rows].astype(F32) + held[at, rows].astype(F32)
+            ).astype(BF16)
             relay.start()
 
     ready = []
     for step in range(chips):
         for at in (chips - 1 - step, step):
             if at not in ready:
-                pair_sum(at)
+                pair_sum((at, 0))
+                pair_sum((at, 1))
                 ready.append(at)
-        at = chips - 1 - step
-        if at > 0:
-            forward(at, at > chip, first_rights[at], rights[at], from_left, chip == 0)
-        at = step
-        if at < chips - 1:
-            forward(at, at < chip, first_lefts[at], lefts[at], from_right, chip == chips - 1)
-    out_ref[...] = held[chip]
+        for part in (0, 1):
+
+            def rightward(at=chips - 1 - step, part=part):
+                if at > 0:
+                    forward((at, part), at > chip, right, from_left, chip == 0)
+
+            def leftward(at=step, part=part):
+                if at < chips - 1:
+                    forward((at, part), at < chip, left, from_right, chip == chips - 1)
+
+            @pl.when(chip < chips // 2)
+            def _():
+                rightward()
+                leftward()
+
+            @pl.when(chip >= chips // 2)
+            def _():
+                leftward()
+                rightward()
 
     for at in range(chips):
 
-        @pl.when((at == chip) & (chip > 0))
+        @pl.when(at == chip)
         def _():
-            rights[at].wait_recv()
-            out_ref[...] = (out_ref[...].astype(F32) + from_left[at].astype(F32)).astype(BF16)
-
-        @pl.when((at == chip) & (chip < chips - 1))
-        def _():
-            lefts[at].wait_recv()
-            out_ref[...] = (out_ref[...].astype(F32) + from_right[at].astype(F32)).astype(BF16)
-
-    for at in range(chips):
-        pairs[at].wait_send()
-        pl.when(at > chip)(rights[at].wait_send)
-        pl.when(at < chip)(lefts[at].wait_send)
+            for part in (0, 1):
+                rows = pl.ds(part * half, half)
+                out_ref[rows] = held[at, rows]
+
+                @pl.when(chip > 0)
+                def _():
+                    right((at, part)).wait_recv()
+                    out_ref[rows] = (
+                        out_ref[rows].astype(F32) + from_left[at, rows].astype(F32)
+                    ).astype(BF16)
+
+                @pl.when(chip < chips - 1)
+                def _():
+                    left((at, part)).wait_recv()
+                    out_ref[rows] = (
+                        out_ref[rows].astype(F32) + from_right[at, rows].astype(F32)
+                    ).astype(BF16)
+
+    for item in items:
+        pair(item).wait_send()
+        pl.when(item[0] > chip)(lambda: right(item).wait_send())
+        pl.when(item[0] < chip)(lambda: left(item).wait_send())
 
 
 def returned(placed):
@@ -553,7 +580,7 @@
         in_specs=[vmem],
         out_specs=vmem,
         scratch_shapes=[pltpu.VMEM((chips, rows, width), BF16)] * 4
-        + [pltpu.SemaphoreType.DMA((3, 2, chips))],
+        + [pltpu.SemaphoreType.DMA((3, 2, 2 * chips))],
         compiler_params=pltpu.CompilerParams(collective_id=1, has_side_effects=True),
         name="return",
     )(placed)

time: 165 us -> 160 us (0.970)
  Pallas kernels: 117 us -> 106 us
  waiting for transfers between devices: 16.5 us -> 22.7 us
    pallas_call x1, Pallas kernels: 35.4 us -> 24.3 us  [returned(): pl.pallas_call(functools.partial(return_kernel, count), out_shape=jax.Sha...]
    reduce_scatter x1, waiting for transfers between devices: 0.02 us -> 6.31 us  [scatter(): return lax.psum_scatter(product, 'tp', scatter_dimension=0, tiled=True)]
  transfers between devices with their start and end apart: 2 -> 2, of which waited for: 1 -> 2; matrix products, arithmetic and copies ran while one was open for 1% -> 1% of each run, Pallas kernels for 33% -> 27%
where the time goes in v3:
time: 160 us
  Pallas kernels  106 us (66%)
  waiting for transfers between devices  22.7 us (14%)
  between operations  14.1 us (9%)
  other arithmetic  6.84 us (4%)
  matrix products  5.35 us (3%)
  local copies, waits for them, and re-layouts  4.65 us (3%)
    pallas_call x1, Pallas kernels, experts(): pl.pallas_call(functools.partial(experts_kernel, tp_count, ep_count), out...  63.5 us
    pallas_call x1, Pallas kernels, returned(): pl.pallas_call(functools.partial(return_kernel, count), out_shape=jax.Sha...  24.3 us
    pallas_call x1, Pallas kernels, block_tables(): pl.pallas_call(tables_kernel, grid=(tokens // BLOCK,), in_specs=[rows] *...  18.1 us
    all_gather x1, waiting for transfers between devices, both_halves(): arrived = lax.all_gather(jnp.concatenate([piece, extra], axis=1), 'ep')  16.4 us
    reduce_scatter x1, waiting for transfers between devices, scatter(): return lax.psum_scatter(product, 'tp', scatter_dimension=0, tiled=True)  6.31 us
  transfers between devices with their start and end apart: 2, of which 2 were waited for; matrix products, arithmetic and copies ran while one was open for 1% of the time, Pallas kernels for 27%

profile of v3, /device:TPU:0, one launch (start us, length us, event | category | flops | bytes accessed | tf_op | source)
XLA Modules:
  0.0 159.7 jit_solution(16380802345434900540)
XLA Ops:
  7.2 0.0 all-gather.3.cloned.1.call-start
  7.2 1.5 multiply_reduce_fusion
  8.7 0.7 reduce_sum.46
  9.4 0.7 broadcast_divide_fusion
  10.1 0.7 select_reduce_fusion.1
  10.8 0.1 copy.27
  11.0 0.7 dynamic_slice.7
  11.7 1.1 multiply_convert_fusion
  12.7 0.7 fusion.9
  13.5 0.0 all-gather.3.cloned.1.call-update
  13.5 0.0 reduce-scatter.2.cloned.1.call-start
  13.6 18.1 %tables.1 = (bf16[256,512]{1,0:T(8,128)(2,1)}, f32[256,512]{1,0:T(8,128)}, bf16[2,2,64,256]{3,2,1,0:T(8,128)(2,1)}) custom-call(bf16[256,512]{1,0:T(8,128)(2,1)} %r_ref.1, bf16[256,512]{1,0:T(8,128)(2,1)} %k_ref.1, bf16[256,512]{1,0:T(8,128)(2,1)} %v_ref.1, bf16[256,512]{1,0:T(8,128)(2,1)} %d_ref.1, bf16[256,512]{1,0:T(8,128)(2,1)} %a_ref.1), custom_call_target="tpu_custom_call" | custom-call | tf_op jit(solution)/shard_map/tables/pallas_call | solution.py:150
  31.7 16.4 %all-gather.3.cloned.1.call-done = bf16[1024,1152]{1,0:T(8,128)(2,1)} async-done(((bf16[128,1152]{1,0:T(8,128)(2,1)}), bf16[1024,1152]{1,0:T(8,128)(2,1)}) %all-gather.3.cloned.1.call-update) | async-done | bytes 2359312 | tf_op jit(solution)/shard_map/all_gather | solution.py:624
  48.1 1.2 multiply_reduce_fusion.1
  49.3 0.1 fusion.14
  49.4 3.2 %fusion.2 = bf16[8,80,1024]{2,1,0:T(8,128)(2,1)} fusion(bf16[8,128,1152]{2,1,0:T(8,128)(2,1)} %bitcast.11, f32[8,128]{1,0:T(8,128)S(1)} %fusion.14, pred[8,128]{1,0:T(8,128)(4,1)S(1)} %broadcast_compare_fusion), kind=kOutput, calls=%fused_computation.4 | convolution fusion | flops 168591360 | bytes 3412992 | tf_op jit(solution)/shard_map/scr,srn->scn/dot_general | solution.py:642
  52.6 0.2 select_reduce_fusion
  52.8 0.9 reshape.58.share_ref
  53.7 63.5 %experts.1 = (bf16[256,4096]{1,0:T(8,128)(2,1)}, bf16[640,1024]{1,0:T(8,128)(2,1)}) custom-call(bf16[640,1024]{1,0:T(8,128)(2,1)} %bitcast.9, bf16[4096,256]{1,0:T(8,128)(2,1)} %bitcast.12, bf16[4096,256]{1,0:T(8,128)(2,1)} %bitcast.13, bf16[1024,1024]{1,0:T(8,128)(2,1)} %bitcast.14, f32[640,1]{1,0:T(8,128)} %reshape.58.share_ref, ...), custom_call_target="tpu_custom_call" | custom-call | tf_op jit(solution)/shard_map/experts/pallas_call | solution.py:403
  117.2 0.0 copy-start
  117.2 0.0 reduce-scatter.2.cloned.1.call-update
  117.2 1.3 copy-done
  118.5 2.1 %convolution_convert_fusion.placed_ref = bf16[8,128,1024]{2,1,0:T(8,128)(2,1)} fusion(bf16[8,80,1024]{2,1,0:T(8,128)(2,1)S(1)} %bitcast.15, f32[8,128]{1,0:T(8,128)S(1)} %fusion.14, pred[8,128]{1,0:T(8,128)(4,1)S(1)} %broadcast_compare_fusion), kind=kOutput, calls=%fused_computation.3 | convolution fusion | flops 168984576 | bytes 3412992 | tf_op jit(solution)/shard_map/scr,scd->srd/dot_general | solution.py:658
  120.6 24.3 %return.1 = bf16[128,1024]{1,0:T(8,128)(2,1)} custom-call(bf16[8,128,1024]{2,1,0:T(8,128)(2,1)} %convolution_convert_fusion.placed_ref), custom_call_target="tpu_custom_call" | custom-call | tf_op jit(solution)/shard_map/return/pallas_call | solution.py:577
  144.9 6.3 %reduce-scatter.2.cloned.1.call-done = bf16[64,4096]{1,0:T(8,128)(2,1)} async-done(((bf16[256,4096]{1,0:T(8,128)(2,1)}), bf16[64,4096]{1,0:T(8,128)(2,1)}) %reduce-scatter.2.cloned.1.call-update) | async-done | bytes 524304 | tf_op jit(solution)/shard_map/reduce_scatter | solution.py:440
  151.2 1.7 %copy.29 = bf16[128,1024]{1,0:T(8,128)(2,1)} copy(bf16[128,1024]{1,0:T(8,128)(2,1)} %return.1) | data formatting | bytes 524288
  (5 shorter events, 0.0 us)
Async XLA Ops:
  7.2 40.9 %all-gather.3.cloned.1.call-start = ((), (), s32[]{:S(2)}) async-start(), calls=%async_computation.2 | async-start | bytes 2654208 | tf_op jit(solution)/shard_map/all_gather | solution.py:624
  13.5 137.7 %reduce-scatter.2.cloned.1.call-start = ((), (), s32[]{:S(2)}) async-start(), calls=%async_computation.1 | async-start | bytes 2621440 | tf_op jit(solution)/shard_map/reduce_scatter | solution.py:440
  117.2 1.3 copy-start
Sparse Core Ops, SparseCore 0:
  13.6 34.3 all-gather.2
  117.4 33.8 reduce-scatter.1
